TPU v7x, 32 devices: a whole 2x2x4 slice. The times are simulated.
32 devices in a mesh: sp: 4 (over y, x), tp: 8 (over z, core).
Axes of the slice: x: 2, y: 2, z: 4, core: 2. Of those that a mesh axis runs over, the one named last changes fastest.
Arguments:
- stream: bfloat16 [2048, 1024], P('sp', 'tp'), may hold values from -6 to 6
- gain_first: bfloat16 [1024], P('tp'), may hold values from 0.099609375 to 1.8984375
- query_first: bfloat16 [1024, 1024], P('sp', 'tp'), may hold values from -0.1875 to 0.1875
- key_first: bfloat16 [1024, 1024], P('sp', 'tp'), may hold values from -0.1875 to 0.1875
- value_first: bfloat16 [1024, 1024], P('sp', 'tp'), may hold values from -0.1875 to 0.1875
- offset_first: float32 [8, 15, 31], P('tp'), may hold values from -4 to 254
- gain_second: bfloat16 [1024], P('tp'), may hold values from 0.099609375 to 1.8984375
- query_second: bfloat16 [1024, 1024], P('sp', 'tp'), may hold values from -0.1875 to 0.1875
- key_second: bfloat16 [1024, 1024], P('sp', 'tp'), may hold values from -0.1875 to 0.1875
- value_second: bfloat16 [1024, 1024], P('sp', 'tp'), may hold values from -0.1875 to 0.1875
- offset_second: float32 [8, 15, 31], P('tp'), may hold values from -4 to 254
Outputs:
- result: bfloat16 [2048, 1024], P('sp', 'tp')
All inputs are finite; a program needn't handle non-finite values.
Results may differ from a plain program's by a relative error of at most 0.008.
Values may be sent and summed in bfloat16 or wider, within the bound.
A program may use at most 64 MiB of HBM per device.

v0:
```python
import functools

import jax
import jax.numpy as jnp
from jax import lax
from jax.experimental import pallas as pl
from jax.experimental.pallas import tpu as pltpu
from jax.sharding import PartitionSpec as P

GRID_W = 64
WIN_R = 8
WIN_C = 16
HALO = 4
BATCH = 4
GAIN_ROWS = 16
epsilon = 1e-06
MESH = pl.DeviceIdType.MESH


def build_bias(table_ref, rows_ref, tiles_ref):
    rows_ref[...] = jnp.zeros_like(rows_ref)
    rows_ref[0 : 2 * WIN_R - 1, 0 : 2 * WIN_C - 1] = table_ref[:, 0, :]
    shape = (GRID_W, 2 * GRID_W)
    column = lax.broadcasted_iota(jnp.int32, shape, 0)
    key_column = lax.broadcasted_iota(jnp.int32, shape, 1)
    key_column = jnp.where(key_column >= GRID_W, key_column - GRID_W, key_column)
    start = jnp.clip(column - WIN_C // 2, 0, GRID_W - WIN_C)
    inside = (key_column >= start) & (key_column < start + WIN_C)
    for o in range(2 * WIN_R - 2):
        pair = rows_ref[o : o + 1, :] + pltpu.roll(rows_ref[o + 1 : o + 2, :], GRID_W, 1)
        tile = pltpu.roll(
            jnp.broadcast_to(pair, shape), 2 * GRID_W - (WIN_C - 1), 1, stride=1, stride_axis=0
        )
        tiles_ref[o] = jnp.where(inside, tile, -1e30)


def kernel(
    n_sp,
    n_tp,
    x_ref,
    gain_a,
    gain_b,
    wq_a,
    wk_a,
    wv_a,
    wq_b,
    wk_b,
    wv_b,
    table_a,
    table_b,
    out_ref,
    xg_a,
    xg_b,
    wkv_a,
    wkv_b,
    wqg_a,
    wqg_b,
    kvp_a,
    kvp_b,
    q_buf,
    normed,
    rows_buf,
    tiles_a,
    tiles_b,
    load_sem,
    xs_sem,
    xf_sem,
    xl_sem,
    xr_sem,
    ws_sem,
    wr_sem,
    hs_sem,
    hr_sem,
):
    sp = lax.axis_index("sp")
    tp = lax.axis_index("tp")
    tokens, feat = x_ref.shape
    depth = wq_a.shape[0]
    rows_dev = tokens // GRID_W
    total_rows = rows_dev * n_sp
    half = n_tp // 2
    core = lax.rem(tp, 2)
    z = tp // 2
    group = rows_dev // 2 if rows_dev % 2 == 0 else 1
    chunk = group * GRID_W
    count = rows_dev // group
    low_half = tuple(range(count // 2, count)) + tuple(range(count // 2))
    orders = (low_half, tuple(range(count)))
    partner = tp + 1 - 2 * core
    low = HALO * GRID_W
    below = (HALO - 1 if rows_dev >= WIN_R else HALO) * GRID_W
    factor = feat ** (-0.5)

    xg = (xg_a, xg_b)
    wkv = (wkv_a, wkv_b)
    wqg = (wqg_a, wqg_b)
    kvp = (kvp_a, kvp_b)
    tiles = (tiles_a, tiles_b)

    def w_rows(device):
        return pl.ds(pl.multiple_of(device * depth, depth), depth)

    mine = w_rows(sp)
    def place(layer, part):
        if layer == 1:
            return part * chunk
        return GAIN_ROWS + orders[0].index(part) * chunk

    loads = [
        (x_ref.at[pl.ds(part * chunk, chunk)], xg_a.at[tp, pl.ds(place(0, part), chunk)])
        for part in orders[0]
    ] + [
        (wk_a, wkv_a.at[mine, pl.ds(0, feat)]),
        (wv_a, wkv_a.at[mine, pl.ds(feat, feat)]),
        (wq_a, wqg_a.at[mine]),
        (wk_b, wkv_b.at[mine, pl.ds(0, feat)]),
        (wv_b, wkv_b.at[mine, pl.ds(feat, feat)]),
        (wq_b, wqg_b.at[mine]),
    ]
    loads = [pltpu.make_async_copy(s, d, load_sem.at[i]) for i, (s, d) in enumerate(loads)]
    for load in loads:
        load.start()
    spare = jnp.zeros((GAIN_ROWS - 2, feat), jnp.float32)
    both = [gain_a[...].astype(jnp.float32), gain_b[...].astype(jnp.float32), spare]
    xg_a[tp, 0:GAIN_ROWS, :] = jnp.concatenate(both, axis=0).astype(jnp.bfloat16)

    barrier = pltpu.get_barrier_semaphore()
    chip_peers = [lax.rem(tp + 2 * k, n_tp) for k in range(1, half)]
    sp_peers = [lax.rem(sp + k, n_sp) for k in range(1, n_sp)]
    sp_sources = [lax.rem(sp + n_sp - k, n_sp) for k in range(1, n_sp)]
    ends = int(half >= 4)
    at_end = (z == 0) | (z == half - 1)
    pl.semaphore_signal(barrier, inc=1, device_id=(sp, partner), device_id_type=MESH)

    def greet(target):
        pl.semaphore_signal(barrier, inc=1, device_id=(sp, target), device_id_type=MESH)

    for k, t in enumerate(chip_peers, 1):
        opposite = ((z == 0) & (k == half - 1)) | ((z == half - 1) & (k == 1))
        if ends:
            pl.when(jnp.logical_not(opposite))(functools.partial(greet, t))
        else:
            greet(t)
    for s in sp_peers:
        pl.semaphore_signal(barrier, inc=1, device_id=(s, tp), device_id_type=MESH)
    pl.semaphore_wait(barrier, half + n_sp - 1 - ends * at_end.astype(jnp.int32))

    def remote(src, dst, send, recv, device):
        return pltpu.make_async_remote_copy(
            src_ref=src,
            dst_ref=dst,
            send_sem=send,
            recv_sem=recv,
            device_id=device,
            device_id_type=MESH,
        )

    sent = []

    def x_copy(layer, part, slot, sem, target):
        at, size = place(layer, part), chunk
        if layer == 0 and part == orders[0][0]:
            at, size = 0, chunk + GAIN_ROWS
        ref = xg[layer].at[slot, pl.ds(at, size)]
        return remote(ref, ref, sem, xr_sem.at[layer, part, slot], (sp, target))

    def begin(copy, condition=None):
        sent.append((copy, condition))
        if condition is None:
            copy.start()
        else:
            pl.when(condition)(copy.start)

    def x_start(layer, part):
        begin(x_copy(layer, part, tp, xf_sem.at[layer, part, tp], partner))
        for k in range(1, half):
            right = z + k <= half - (1 if k <= 2 else 2)
            left = z - k >= (0 if k <= 2 else 1)
            sem = xs_sem.at[layer, part, k]
            begin(x_copy(layer, part, tp, sem, tp + 2 * k), right)
            sem = xs_sem.at[layer, part, half + k]
            begin(x_copy(layer, part, tp, sem, tp - 2 * k), left)

    def x_finish(layer, part):
        near = 1 - 2 * ((2 * z) // half)
        for k in range(1, half):
            slot = lax.rem(tp + n_tp + 2 * k * near, n_tp)
            relay = xl_sem.at[layer, part, slot]
            x_copy(layer, part, slot, relay, partner).wait_recv()
            right = x_copy(layer, part, slot, relay, tp + 2)
            begin(right, (slot < tp - 3) & (z == half - 2))
            left = x_copy(layer, part, slot, relay, tp - 2)
            begin(left, (slot > tp + 3) & (z == 1))
            begin(x_copy(layer, part, slot, xf_sem.at[layer, part, slot], partner))
        for k in range(half):
            slot = lax.rem(partner + n_tp + 2 * k * near, n_tp)
            x_copy(layer, part, slot, xf_sem.at[layer, part, slot], partner).wait_recv()

    def w_copy(layer, which, slot, index, target):
        ref = (wkv, wqg)[which][layer].at[w_rows(slot)]
        return remote(
            ref, ref, ws_sem.at[layer, which, index], wr_sem.at[layer, which, slot], (target, tp)
        )

    def w_start(layer, which):
        for index, target in enumerate(sp_peers):
            begin(w_copy(layer, which, sp, index, target))

    def w_finish(layer, which):
        for slot in sp_sources:
            w_copy(layer, which, slot, 0, slot).wait_recv()

    def down(layer):
        buf = kvp[layer]
        return remote(
            buf.at[pl.ds(tokens, low)],
            buf.at[pl.ds(0, low)],
            hs_sem.at[layer, 0],
            hr_sem.at[layer, 0],
            (lax.rem(sp + 1, n_sp), tp),
        )

    def up(layer):
        buf = kvp[layer]
        return remote(
            buf.at[pl.ds(low, below)],
            buf.at[pl.ds(low + tokens, below)],
            hs_sem.at[layer, 1],
            hr_sem.at[layer, 1],
            (lax.rem(sp + n_sp - 1, n_sp), tp),
        )

    has_next = sp < n_sp - 1
    has_previous = sp > 0

    def norm(layer, part):
        buf = xg[layer]
        for c in range(group):
            at = pl.ds(place(layer, part) + c * GRID_W, GRID_W)
            to = pl.ds(part * chunk + c * GRID_W, GRID_W)
            total = jnp.zeros((GRID_W, feat), jnp.float32)
            for s in range(n_tp):
                wide = buf[s, at, :].astype(jnp.float32)
                total = total + wide * wide
            mean = jnp.sum(total, axis=-1, keepdims=True) * (1.0 / (n_tp * feat))
            scale = lax.rsqrt(mean + epsilon)
            for s in range(n_tp):
                gain = xg_a[s, 0:GAIN_ROWS, :][layer : layer + 1, :]
                wide = buf[s, at, :].astype(jnp.float32)
                normed[to, s * feat : (s + 1) * feat] = (
                    wide * scale * gain.astype(jnp.float32)
                ).astype(jnp.bfloat16)

    def project(weights, dst, offset, part):
        made = jnp.dot(
            normed[part * chunk : (part + 1) * chunk, :],
            weights[...],
            preferred_element_type=jnp.float32,
        )
        dst[pl.ds(offset + part * chunk, chunk), :] = made.astype(jnp.bfloat16)

    def attend(layer, indices):
        places, scores = [], []
        for index in indices:
            row = sp * rows_dev + index
            first = jnp.minimum(jnp.maximum(row - HALO, 0), total_rows - WIN_R)
            local = first - sp * rows_dev + HALO
            base = first - row + WIN_R - 1
            at = pl.ds(pl.multiple_of(local * GRID_W, GRID_W), WIN_R * GRID_W)
            query = q_buf[index * GRID_W : (index + 1) * GRID_W, :]
            raw = lax.dot_general(
                query,
                kvp[layer][at, 0:feat],
                (((1,), (1,)), ((), ())),
                preferred_element_type=jnp.float32,
            )
            bias = jnp.concatenate([tiles[layer][base + 2 * j] for j in range(WIN_R // 2)], axis=1)
            places.append(at)
            scores.append(raw * factor + bias)
        tops = [jnp.max(score, axis=-1, keepdims=True) for score in scores]
        weights = [jnp.exp(score - top) for score, top in zip(scores, tops)]
        scales = [1.0 / jnp.sum(weight, axis=-1, keepdims=True) for weight in weights]
        outs = [
            jnp.dot(
                (weight * scale).astype(jnp.bfloat16),
                kvp[layer][at, feat : 2 * feat],
                preferred_element_type=jnp.float32,
            )
            for weight, scale, at in zip(weights, scales, places)
        ]
        made = []
        for index, out in zip(indices, outs):
            start = place(layer, index // group) + index % group * GRID_W
            wide = xg[layer][tp, pl.ds(start, GRID_W), :].astype(jnp.float32)
            made.append((wide + out).astype(jnp.bfloat16))
        return made

    for load, part in zip(loads, orders[0]):
        load.wait()
        x_start(0, part)
    rest = loads[count:]
    rest[0].wait()
    rest[1].wait()
    w_start(0, 0)
    rest[2].wait()
    w_start(0, 1)
    build_bias(table_a, rows_buf, tiles_a)
    build_bias(table_b, rows_buf, tiles_b)
    for load in rest[3:]:
        load.wait()

    top_rows = [i for i in range(rows_dev) if i < HALO]
    end_rows = [i for i in range(rows_dev) if i + HALO > rows_dev]
    up_parts = {i // group for i in range(below // GRID_W)}
    down_parts = {i // group for i in range(rows_dev - HALO, rows_dev)}

    for layer in range(2):
        done = set()
        for part in orders[layer]:
            x_finish(layer, part)
            norm(layer, part)
            if not done:
                w_finish(layer, 0)
            project(wkv[layer], kvp[layer], low, part)
            before = set(done)
            done.add(part)
            if down_parts <= done and not down_parts <= before:
                pl.when(has_next)(down(layer).start)
            if up_parts <= done and not up_parts <= before:
                pl.when(has_previous)(up(layer).start)
        if layer == 0:
            w_start(1, 0)
            w_start(1, 1)
        w_finish(layer, 1)
        for part in orders[layer]:
            project(wqg[layer], q_buf, 0, part)

        late = end_rows if layer == 0 else top_rows
        early = top_rows if layer == 0 else end_rows
        early = [i for i in early if i not in late]
        inner = [i for i in range(rows_dev) if i not in late and i not in early]
        finished = set()
        for rows, wait in ((inner, None), (early, layer == 0), (late, layer == 1)):
            if wait is True:
                pl.when(has_previous)(down(layer).wait_recv)
            if wait is False:
                pl.when(has_next)(up(layer).wait_recv)
            for index in rows:
                if (index - rows[0]) % BATCH == 0:
                    batch = [i for i in rows if index <= i < index + BATCH]
                    results = dict(zip(batch, attend(layer, batch)))
                here = pl.ds(index * GRID_W, GRID_W)
                if layer == 1:
                    out_ref[here, :] = results[index]
                    continue
                xg_b[tp, here, :] = results[index]
                finished.add(index)
                part = index // group
                if all(part * group + i in finished for i in range(group)):
                    x_start(1, part)

    for layer in range(2):
        pl.when(has_next)(down(layer).wait_send)
        pl.when(has_previous)(up(layer).wait_send)
    for copy, condition in sent:
        if condition is None:
            copy.wait_send()
        else:
            pl.when(condition)(copy.wait_send)


def body(n_sp, n_tp, stream, gain_a, wq_a, wk_a, wv_a, table_a, gain_b, wq_b, wk_b, wv_b, table_b):
    tokens, feat = stream.shape
    depth = wq_a.shape[0] * n_sp
    rows_dev = tokens // GRID_W
    parts = 2 if rows_dev % 2 == 0 else rows_dev
    bf16 = jnp.bfloat16
    padded = tokens + 2 * HALO * GRID_W
    hbm = pl.BlockSpec(memory_space=pl.ANY)
    vmem = pl.BlockSpec(memory_space=pltpu.VMEM)
    dma = pltpu.SemaphoreType.DMA
    return pl.pallas_call(
        functools.partial(kernel, n_sp, n_tp),
        out_shape=pltpu.VMEM((tokens, feat), bf16),
        in_specs=[hbm] + [vmem] * 2 + [hbm] * 6 + [vmem] * 2,
        out_specs=vmem,
        scratch_shapes=[
            pltpu.VMEM((n_tp, tokens + GAIN_ROWS, feat), bf16),
            pltpu.VMEM((n_tp, tokens, feat), bf16),
            pltpu.VMEM((depth, 2 * feat), bf16),
            pltpu.VMEM((depth, 2 * feat), bf16),
            pltpu.VMEM((depth, feat), bf16),
            pltpu.VMEM((depth, feat), bf16),
            pltpu.VMEM((padded, 2 * feat), bf16),
            pltpu.VMEM((padded, 2 * feat), bf16),
            pltpu.VMEM((tokens, feat), bf16),
            pltpu.VMEM((tokens, n_tp * feat), bf16),
            pltpu.VMEM((2 * WIN_R, 2 * GRID_W), jnp.float32),
            pltpu.VMEM((2 * WIN_R - 2, GRID_W, 2 * GRID_W), jnp.float32),
            pltpu.VMEM((2 * WIN_R - 2, GRID_W, 2 * GRID_W), jnp.float32),
            dma((parts + 6,)),
            dma((2, parts, n_tp)),
            dma((2, parts, n_tp)),
            dma((2, parts, n_tp)),
            dma((2, parts, n_tp)),
            dma((2, 2, n_sp)),
            dma((2, 2, n_sp)),
            dma((2, 2)),
            dma((2, 2)),
        ],
        compiler_params=pltpu.CompilerParams(collective_id=0, has_side_effects=True),
    )(
        stream,
        gain_a.reshape(1, feat),
        gain_b.reshape(1, feat),
        wq_a,
        wk_a,
        wv_a,
        wq_b,
        wk_b,
        wv_b,
        jnp.transpose(table_a, (1, 0, 2)),
        jnp.transpose(table_b, (1, 0, 2)),
    )


def solution(mesh):
    placed = (
        P("sp", "tp"),
        P("tp"),
        P("sp", "tp"),
        P("sp", "tp"),
        P("sp", "tp"),
        P("tp", None, None),
        P("tp"),
        P("sp", "tp"),
        P("sp", "tp"),
        P("sp", "tp"),
        P("tp", None, None),
    )
    return jax.shard_map(
        functools.partial(body, mesh.shape["sp"], mesh.shape["tp"]),
        mesh=mesh,
        in_specs=placed,
        out_specs=P("sp", "tp"),
        check_vma=False,
    )
```

profile of v0, /device:TPU:5, one launch (start us, length us, event | category | flops | bytes accessed | tf_op | source)
XLA Modules:
  0.0 41.1 jit_solution(1022587538571537198)
XLA Ops:
  0.0 40.5 %shard_map.109 = bf16[512,128]{1,0:T(8,128)(2,1)S(1)} custom-call(bf16[512,128]{1,0:T(8,128)(2,1)} %x_ref.1, bf16[1,128]{1,0:T(2,128)(2,1)} %bitcast.6, bf16[1,128]{1,0:T(2,128)(2,1)} %bitcast.7, bf16[256,128]{1,0:T(8,128)(2,1)} %wq_a.1, bf16[256,128]{1,0:T(8,128)(2,1)} %wk_a.1, bf16[256,128]{1,0:T(8,128)(2,1)} %wv_a.1, bf16[256,128]{1,0:T(8,128)(2,1)} %wq_b.1, ...), custom_call_target="tpu_custom_call" | custom-call | tf_op jit(solution)/shard_map/pallas_call | solution.py:382
  40.5 0.7 %copy.13 = bf16[512,128]{1,0:T(8,128)(2,1)} copy(bf16[512,128]{1,0:T(8,128)(2,1)S(1)} %shard_map.109) | data formatting | bytes 262144
where the time goes:
time: 41.3 us; the launch traced here: 41.1 us
  Pallas kernels  40.5 us (98%)
  local copies, waits for them, and re-layouts  0.66 us (2%)
    pallas_call x1, Pallas kernels, body(): pl.pallas_call(functools.partial(kernel, n_sp, n_tp), out_shape=pltpu.VME...  40.5 us

commit v1 on v0

v1 whole, which is shorter than its diff:
```python
import functools

import jax
import jax.numpy as jnp
from jax import lax
from jax.experimental import pallas as pl
from jax.experimental.pallas import tpu as pltpu
from jax.sharding import PartitionSpec as P

GRID_W = 64
WIN_R = 8
WIN_C = 16
HALO = 4
GAIN_ROWS = 16
LAG = 2
BATCH = (4, 4)
QUERY_AT = (3, 0)
W_AFTER = 0
epsilon = 1e-06
MESH = pl.DeviceIdType.MESH


def build_bias(table_ref, rows_ref, tiles_ref):
    rows_ref[...] = jnp.zeros_like(rows_ref)
    rows_ref[0 : 2 * WIN_R - 1, 0 : 2 * WIN_C - 1] = table_ref[:, 0, :]
    shape = (GRID_W, 2 * GRID_W)
    column = lax.broadcasted_iota(jnp.int32, shape, 0)
    key_column = lax.broadcasted_iota(jnp.int32, shape, 1)
    key_column = jnp.where(key_column >= GRID_W, key_column - GRID_W, key_column)
    start = jnp.clip(column - WIN_C // 2, 0, GRID_W - WIN_C)
    inside = (key_column >= start) & (key_column < start + WIN_C)
    for o in range(2 * WIN_R - 2):
        pair = rows_ref[o : o + 1, :] + pltpu.roll(rows_ref[o + 1 : o + 2, :], GRID_W, 1)
        tile = pltpu.roll(
            jnp.broadcast_to(pair, shape), 2 * GRID_W - (WIN_C - 1), 1, stride=1, stride_axis=0
        )
        tiles_ref[o] = jnp.where(inside, tile, -1e30)


def row_orders(rows_dev):
    last = rows_dev - HALO - 1 if rows_dev >= WIN_R else -1
    high = [(r, min(2, rows_dev - r)) for r in range(rows_dev - HALO, rows_dev, 2)]
    low = [(r, min(2, last - r)) for r in range(0, last, 2)]
    if last < 0:
        low = [(r, min(2, rows_dev - HALO - r)) for r in range(0, rows_dev - HALO, 2)]
        return (low + high, high + low)
    return (low + high + [(last, 1)], high + low + [(last, 1)])


def kernel(
    n_sp,
    n_tp,
    x_ref,
    gain_a,
    gain_b,
    wq_a,
    wk_a,
    wv_a,
    wq_b,
    wk_b,
    wv_b,
    table_a,
    table_b,
    out_ref,
    xg_a,
    xg_b,
    wkv_a,
    wkv_b,
    wqg_a,
    wqg_b,
    kvp_a,
    kvp_b,
    q_buf,
    normed,
    rows_buf,
    tiles_a,
    tiles_b,
    load_sem,
    xs_sem,
    xr_sem,
    xp_sem,
    ws_sem,
    wr_sem,
    hs_sem,
    hr_sem,
):
    sp = lax.axis_index("sp")
    tp = lax.axis_index("tp")
    tokens, feat = x_ref.shape
    depth = wq_a.shape[0]
    rows_dev = tokens // GRID_W
    total_rows = rows_dev * n_sp
    half = n_tp // 2
    core = lax.rem(tp, 2)
    z = tp // 2
    partner = tp + 1 - 2 * core
    low = HALO * GRID_W
    below_rows = HALO - 1 if rows_dev >= WIN_R else HALO
    below = below_rows * GRID_W
    factor = feat ** (-0.5)
    orders = row_orders(rows_dev)
    chunks = len(orders[0])

    xg = (xg_a, xg_b)
    wkv = (wkv_a, wkv_b)
    wqg = (wqg_a, wqg_b)
    kvp = (kvp_a, kvp_b)
    tiles = (tiles_a, tiles_b)

    sp_peers = [lax.rem(sp + k, n_sp) for k in range(1, n_sp)]
    has_next = sp < n_sp - 1
    has_previous = sp > 0
    has_right = z < half - 1
    has_left = z > 0

    barrier = pltpu.get_barrier_semaphore()

    def greet(s, t):
        pl.semaphore_signal(barrier, inc=1, device_id=(s, t), device_id_type=MESH)

    pl.when(has_right)(lambda: greet(sp, tp + 2))
    pl.when(has_left)(lambda: greet(sp, tp - 2))
    for s in sp_peers:
        greet(s, tp)
    greet(sp, partner)

    def slot_of(c, j):
        return c * half + j

    own = slot_of(core, z)

    def w_rows(device):
        return pl.ds(pl.multiple_of(device * depth, depth), depth)

    mine = w_rows(sp)

    def place(layer, row):
        at = GAIN_ROWS if layer == 0 else 0
        for first, size in orders[layer]:
            if first <= row < first + size:
                return at + (row - first) * GRID_W
            at += size * GRID_W

    def span(layer, c):
        first, size = orders[layer][c]
        at, size = place(layer, first), size * GRID_W
        if layer == 0 and c == 0:
            return pl.ds(0, size + GAIN_ROWS)
        return pl.ds(at, size)

    runs = []
    for first, size in orders[0]:
        if runs and sum(runs[-1]) == first:
            runs[-1] = (runs[-1][0], runs[-1][1] + size)
        else:
            runs.append((first, size))
    for first, size in runs:
        pltpu.make_async_copy(
            x_ref.at[pl.ds(first * GRID_W, size * GRID_W)],
            xg_a.at[own, pl.ds(place(0, first), size * GRID_W)],
            load_sem.at[0],
        ).start()
    loads = (
        (1, wk_a, wkv_a.at[mine, pl.ds(0, feat)]),
        (1, wv_a, wkv_a.at[mine, pl.ds(feat, feat)]),
        (2, wq_a, wqg_a.at[mine]),
        (3, wk_b, wkv_b.at[mine, pl.ds(0, feat)]),
        (3, wv_b, wkv_b.at[mine, pl.ds(feat, feat)]),
        (4, wq_b, wqg_b.at[mine]),
    )
    for i, src, dst in loads:
        pltpu.make_async_copy(src, dst, load_sem.at[i]).start()

    def loaded(i, ref):
        pltpu.make_async_copy(ref, ref, load_sem.at[i]).wait()

    spare = jnp.zeros((GAIN_ROWS - 2, feat), jnp.float32)
    both = [gain_a[...].astype(jnp.float32), gain_b[...].astype(jnp.float32), spare]
    xg_a[own, 0:GAIN_ROWS, :] = jnp.concatenate(both, axis=0).astype(jnp.bfloat16)

    def remote(src, dst, send, recv, device):
        return pltpu.make_async_remote_copy(
            src_ref=src,
            dst_ref=dst,
            send_sem=send,
            recv_sem=recv,
            device_id=device,
            device_id_type=MESH,
        )

    def x_copy(layer, c, j, target):
        ref = xg[layer].at[slot_of(core, j), span(layer, c)]
        index = lax.rem(j - target + half, half) - 1
        device = (sp, 2 * target + core)
        return remote(ref, ref, xs_sem.at[layer], xr_sem.at[layer, c, index], device)

    def x_pass(layer, c, j):
        ref = xg[layer].at[slot_of(core, j), span(layer, c)]
        return remote(ref, ref, xs_sem.at[layer], xp_sem.at[layer, c], (sp, partner))

    def x_start(layer, c):
        pl.when(has_right)(lambda: x_copy(layer, c, z, z + 1).start())
        pl.when(has_left)(lambda: x_copy(layer, c, z, z - 1).start())
        x_pass(layer, c, z).start()

    both_sides = jnp.minimum(z, half - 1 - z)
    far = jnp.where(2 * z < half, 1, -1)

    def source(k):
        paired = k <= 2 * both_sides
        away = jnp.where(paired, (k + 1) // 2, k - both_sides)
        side = jnp.where(paired, 1 if k % 2 else -1, far)
        return z + away * side, side

    sources = [source(k) for k in range(1, half)]

    def x_take(layer, c, k):
        j, side = sources[k - 1]
        index = lax.rem(j - z + half, half) - 1
        ref = xg[layer].at[slot_of(core, j), span(layer, c)]
        remote(ref, ref, xs_sem.at[layer], xr_sem.at[layer, c, index], (sp, partner)).wait_recv()
        onward = jnp.where(side > 0, has_left, has_right)
        pl.when(onward)(lambda: x_copy(layer, c, j, z - side).start())
        x_pass(layer, c, j).start()

    def x_finish(layer, c):
        ref = xg[layer].at[pl.ds((1 - core) * half, half), span(layer, c)]
        remote(ref, ref, xs_sem.at[layer], xp_sem.at[layer, c], (sp, partner)).wait_recv()

    def x_sent(layer, counts):
        for count in counts:
            ref = xg[layer].at[pl.ds(0, count)]
            remote(ref, ref, xs_sem.at[layer], xp_sem.at[layer, 0], (sp, partner)).wait_send()

    def x_drain(layer):
        for at in range(half):
            count = half
            count += at + 1 if at < half - 1 else 0
            count += half - at if at > 0 else 0
            counts = [n_tp] * (count // n_tp) + [count % n_tp] * (count % n_tp > 0)
            pl.when(z == at)(functools.partial(x_sent, layer, counts))

    def w_copy(layer, which, slot, target):
        ref = (wkv, wqg)[which][layer].at[w_rows(slot)]
        return remote(ref, ref, ws_sem.at[layer, which], wr_sem.at[layer, which], (target, tp))

    def w_start(layer, which):
        for target in sp_peers:
            w_copy(layer, which, sp, target).start()

    def w_all(layer, which):
        ref = (wkv, wqg)[which][layer].at[pl.ds(0, (n_sp - 1) * depth)]
        return remote(ref, ref, ws_sem.at[layer, which], wr_sem.at[layer, which], (sp, partner))

    def halo(layer, way, src, dst, size):
        buf = kvp[layer]
        target = lax.rem(sp + 1, n_sp) if way == 0 else lax.rem(sp + n_sp - 1, n_sp)
        return remote(
            buf.at[pl.ds(src, size)],
            buf.at[pl.ds(dst, size)],
            hs_sem.at[layer, way],
            hr_sem.at[layer, way],
            (target, tp),
        )

    def halo_start(layer, first, size):
        start = max(first, rows_dev - HALO)
        if start < first + size:
            src = low + start * GRID_W
            rows = (first + size - start) * GRID_W
            pl.when(has_next)(lambda: halo(layer, 0, src, src - tokens, rows).start())
        stop = min(first + size, below_rows)
        if first < stop:
            src = low + first * GRID_W
            rows = (stop - first) * GRID_W
            pl.when(has_previous)(lambda: halo(layer, 1, src, src + tokens, rows).start())

    def halo_all(layer, way):
        at, size = ((0, low), (low + tokens, below))[way]
        return halo(layer, way, at, at, size)

    def norm(layer, c):
        buf = xg[layer]
        first, size = orders[layer][c]
        for row in range(first, first + size):
            at = pl.ds(place(layer, row), GRID_W)
            to = pl.ds(row * GRID_W, GRID_W)
            total = jnp.zeros((GRID_W, feat), jnp.float32)
            for s in range(n_tp):
                wide = buf[s, at, :].astype(jnp.float32)
                total = total + wide * wide
            mean = jnp.sum(total, axis=-1, keepdims=True) * (1.0 / (n_tp * feat))
            scale = lax.rsqrt(mean + epsilon)
            for s in range(n_tp):
                slot = slot_of(s % 2, s // 2)
                gain = xg_a[slot, 0:GAIN_ROWS, :][layer : layer + 1, :]
                wide = buf[slot, at, :].astype(jnp.float32)
                normed[to, s * feat : (s + 1) * feat] = (
                    wide * scale * gain.astype(jnp.float32)
                ).astype(jnp.bfloat16)

    def project(weights, dst, offset, first, size):
        at, rows = first * GRID_W, size * GRID_W
        made = jnp.dot(
            normed[at : at + rows, :], weights[...], preferred_element_type=jnp.float32
        )
        dst[pl.ds(offset + at, rows), :] = made.astype(jnp.bfloat16)

    def attend(layer, indices):
        places, scores = [], []
        for index in indices:
            row = sp * rows_dev + index
            first = jnp.minimum(jnp.maximum(row - HALO, 0), total_rows - WIN_R)
            local = first - sp * rows_dev + HALO
            base = first - row + WIN_R - 1
            at = pl.ds(pl.multiple_of(local * GRID_W, GRID_W), WIN_R * GRID_W)
            query = q_buf[index * GRID_W : (index + 1) * GRID_W, :]
            raw = lax.dot_general(
                query,
                kvp[layer][at, 0:feat],
                (((1,), (1,)), ((), ())),
                preferred_element_type=jnp.float32,
            )
            bias = jnp.concatenate([tiles[layer][base + 2 * j] for j in range(WIN_R // 2)], axis=1)
            places.append(at)
            scores.append(raw * factor + bias)
        tops = [jnp.max(score, axis=-1, keepdims=True) for score in scores]
        weights = [jnp.exp(score - top) for score, top in zip(scores, tops)]
        scales = [1.0 / jnp.sum(weight, axis=-1, keepdims=True) for weight in weights]
        outs = [
            jnp.dot(
                (weight * scale).astype(jnp.bfloat16),
                kvp[layer][at, feat : 2 * feat],
                preferred_element_type=jnp.float32,
            )
            for weight, scale, at in zip(weights, scales, places)
        ]
        made = []
        for index, out in zip(indices, outs):
            wide = xg[layer][own, pl.ds(place(layer, index), GRID_W), :].astype(jnp.float32)
            made.append((wide + out).astype(jnp.bfloat16))
        return made

    sync = 1 + (n_sp - 1) + has_right.astype(jnp.int32) + has_left.astype(jnp.int32)
    pl.semaphore_wait(barrier, sync)
    loaded(0, xg_a.at[own, pl.ds(GAIN_ROWS, tokens)])
    for c in range(chunks):
        x_start(0, c)
    loaded(1, wkv_a.at[mine])
    w_start(0, 0)
    loaded(2, wqg_a.at[mine])
    w_start(0, 1)
    build_bias(table_a, rows_buf, tiles_a)
    build_bias(table_b, rows_buf, tiles_b)
    loaded(3, wkv_b.at[mine])
    loaded(4, wqg_b.at[mine])

    high_rows = list(range(rows_dev - HALO, rows_dev))
    low_rows = [i for i in range(rows_dev) if i not in high_rows]
    for layer in range(2):
        last = half - 1
        early = [(k, k + 1) for k in range(1, last - 1, 2)]
        rest = list(range(2 * len(early) + 1, last))
        for group in early + [(k,) for k in rest]:
            for c in range(chunks):
                for k in group:
                    x_take(layer, c, k)
        ready = QUERY_AT[layer]
        for c in range(chunks + LAG):
            if c < chunks:
                x_take(layer, c, last)
            if c < LAG:
                continue
            x_finish(layer, c - LAG)
            norm(layer, c - LAG)
            if c == LAG:
                w_all(layer, 0).wait_recv()
            first, size = orders[layer][c - LAG]
            project(wkv[layer], kvp[layer], low, first, size)
            halo_start(layer, first, size)
            if c - LAG == min(ready, chunks - 1):
                w_all(layer, 1).wait_recv()
                for part in orders[layer][: c - LAG + 1]:
                    project(wqg[layer], q_buf, 0, *part)
            elif c - LAG > ready:
                project(wqg[layer], q_buf, 0, first, size)

        groups = ((1, high_rows), (0, low_rows)) if layer == 0 else ((0, low_rows), (1, high_rows))
        if rows_dev < WIN_R:
            groups = ((0, []), (1, high_rows), (0, low_rows))
        waited, finished, sent = set(), set(), 0
        for way, rows in groups:
            if way not in waited:
                waited.add(way)
                pl.when((has_next, has_previous)[1 - way])(halo_all(layer, way).wait_recv)
            for at in range(0, len(rows), BATCH[layer]):
                batch = rows[at : at + BATCH[layer]]
                for index, made in zip(batch, attend(layer, batch)):
                    if layer == 1:
                        out_ref[index * GRID_W : (index + 1) * GRID_W, :] = made
                    else:
                        xg_b[own, pl.ds(place(1, index), GRID_W), :] = made
                        finished.add(index)
                while layer == 0 and sent < chunks:
                    first, size = orders[1][sent]
                    if not set(range(first, first + size)) <= finished:
                        break
                    x_start(1, sent)
                    sent += 1
            if layer == 0 and way == W_AFTER:
                w_start(1, 0)
                w_start(1, 1)

    for layer in range(2):
        pl.when(has_next)(halo_all(layer, 0).wait_send)
        pl.when(has_previous)(halo_all(layer, 1).wait_send)
        w_all(layer, 0).wait_send()
        w_all(layer, 1).wait_send()
        x_drain(layer)


def body(n_sp, n_tp, stream, gain_a, wq_a, wk_a, wv_a, table_a, gain_b, wq_b, wk_b, wv_b, table_b):
    tokens, feat = stream.shape
    depth = wq_a.shape[0] * n_sp
    rows_dev = tokens // GRID_W
    chunks = len(row_orders(rows_dev)[0])
    bf16 = jnp.bfloat16
    padded = tokens + 2 * HALO * GRID_W
    hbm = pl.BlockSpec(memory_space=pl.ANY)
    vmem = pl.BlockSpec(memory_space=pltpu.VMEM)
    dma = pltpu.SemaphoreType.DMA
    return pl.pallas_call(
        functools.partial(kernel, n_sp, n_tp),
        out_shape=pltpu.VMEM((tokens, feat), bf16),
        in_specs=[hbm] + [vmem] * 2 + [hbm] * 6 + [vmem] * 2,
        out_specs=vmem,
        scratch_shapes=[
            pltpu.VMEM((n_tp, tokens + GAIN_ROWS, feat), bf16),
            pltpu.VMEM((n_tp, tokens, feat), bf16),
            pltpu.VMEM((depth, 2 * feat), bf16),
            pltpu.VMEM((depth, 2 * feat), bf16),
            pltpu.VMEM((depth, feat), bf16),
            pltpu.VMEM((depth, feat), bf16),
            pltpu.VMEM((padded, 2 * feat), bf16),
            pltpu.VMEM((padded, 2 * feat), bf16),
            pltpu.VMEM((tokens, feat), bf16),
            pltpu.VMEM((tokens, n_tp * feat), bf16),
            pltpu.VMEM((2 * WIN_R, 2 * GRID_W), jnp.float32),
            pltpu.VMEM((2 * WIN_R - 2, GRID_W, 2 * GRID_W), jnp.float32),
            pltpu.VMEM((2 * WIN_R - 2, GRID_W, 2 * GRID_W), jnp.float32),
            dma((5,)),
            dma((2,)),
            dma((2, chunks, n_tp // 2 - 1)),
            dma((2, chunks)),
            dma((2, 2)),
            dma((2, 2)),
            dma((2, 2)),
            dma((2, 2)),
        ],
        compiler_params=pltpu.CompilerParams(collective_id=0, has_side_effects=True),
    )(
        stream,
        gain_a.reshape(1, feat),
        gain_b.reshape(1, feat),
        wq_a,
        wk_a,
        wv_a,
        wq_b,
        wk_b,
        wv_b,
        jnp.transpose(table_a, (1, 0, 2)),
        jnp.transpose(table_b, (1, 0, 2)),
    )


def solution(mesh):
    placed = (
        P("sp", "tp"),
        P("tp"),
        P("sp", "tp"),
        P("sp", "tp"),
        P("sp", "tp"),
        P("tp", None, None),
        P("tp"),
        P("sp", "tp"),
        P("sp", "tp"),
        P("sp", "tp"),
        P("tp", None, None),
    )
    return jax.shard_map(
        functools.partial(body, mesh.shape["sp"], mesh.shape["tp"]),
        mesh=mesh,
        in_specs=placed,
        out_specs=P("sp", "tp"),
        check_vma=False,
    )
```

time: 41.3 us -> 43.3 us (1.048)
  the two profiles are of different devices: /device:TPU:5 before, /device:TPU:0 now
where the time goes in v1:
time: 43.3 us; the launch traced here: 43.1 us
  Pallas kernels  42.5 us (98%)
  local copies, waits for them, and re-layouts  0.66 us (2%)
    pallas_call x1, Pallas kernels, body(): pl.pallas_call(functools.partial(kernel, n_sp, n_tp), out_shape=pltpu.VME...  42.5 us

profile of v1, /device:TPU:0, one launch (start us, length us, event | category | flops | bytes accessed | tf_op | source)
XLA Modules:
  0.0 43.1 jit_solution(15918806360471274547)
XLA Ops:
  0.0 42.5 %shard_map.109 = bf16[512,128]{1,0:T(8,128)(2,1)S(1)} custom-call(bf16[512,128]{1,0:T(8,128)(2,1)} %x_ref.1, bf16[1,128]{1,0:T(2,128)(2,1)} %bitcast.6, bf16[1,128]{1,0:T(2,128)(2,1)} %bitcast.7, bf16[256,128]{1,0:T(8,128)(2,1)} %wq_a.1, bf16[256,128]{1,0:T(8,128)(2,1)} %wk_a.1, bf16[256,128]{1,0:T(8,128)(2,1)} %wv_a.1, bf16[256,128]{1,0:T(8,128)(2,1)} %wq_b.1, ...), custom_call_target="tpu_custom_call" | custom-call | tf_op jit(solution)/shard_map/pallas_call | solution.py:432
  42.5 0.7 %copy.13 = bf16[512,128]{1,0:T(8,128)(2,1)} copy(bf16[512,128]{1,0:T(8,128)(2,1)S(1)} %shard_map.109) | data formatting | bytes 262144

commit v2 on v1

v2 whole, which is shorter than its diff:
```python
import functools

import jax
import jax.numpy as jnp
from jax import lax
from jax.experimental import pallas as pl
from jax.experimental.pallas import tpu as pltpu
from jax.sharding import PartitionSpec as P

GRID_W = 64
WIN_R = 8
WIN_C = 16
HALO = 4
GAIN_ROWS = 16
LAG = (1, 1)
DIRECT = (0, 4)
DEFER = ((0, 0, 0, 0), (1, 2, 3, 0))
BATCH = 4
W_STEP = 2
epsilon = 1e-06
MESH = pl.DeviceIdType.MESH


def build_bias(table_ref, rows_ref, tiles_ref):
    rows_ref[...] = jnp.zeros_like(rows_ref)
    rows_ref[0 : 2 * WIN_R - 1, 0 : 2 * WIN_C - 1] = table_ref[:, 0, :]
    shape = (GRID_W, 2 * GRID_W)
    column = lax.broadcasted_iota(jnp.int32, shape, 0)
    key_column = lax.broadcasted_iota(jnp.int32, shape, 1)
    key_column = jnp.where(key_column >= GRID_W, key_column - GRID_W, key_column)
    start = jnp.clip(column - WIN_C // 2, 0, GRID_W - WIN_C)
    inside = (key_column >= start) & (key_column < start + WIN_C)
    for o in range(2 * WIN_R - 2):
        pair = rows_ref[o : o + 1, :] + pltpu.roll(rows_ref[o + 1 : o + 2, :], GRID_W, 1)
        tile = pltpu.roll(
            jnp.broadcast_to(pair, shape), 2 * GRID_W - (WIN_C - 1), 1, stride=1, stride_axis=0
        )
        tiles_ref[o] = jnp.where(inside, tile, -1e30)


def row_orders(rows_dev):
    if rows_dev < WIN_R:
        each = [[r] for r in range(rows_dev)]
        return (each, each)
    edge, last = rows_dev - HALO, rows_dev - 1
    inner = list(range(HALO - 1, edge))
    first = [[0, last], [1, last - 1], [2, last - 2], inner + [edge]]
    second = [inner + [edge, edge + 1], [2, last - 1], [1, last], [0]]
    return (first, second)


def halo_plan(rows_dev, layer):
    below = HALO - 1 if rows_dev >= WIN_R else HALO
    edge, plan = rows_dev - HALO, []
    for chunk in row_orders(rows_dev)[layer]:
        up = [(1, row) for row in chunk if row < below]
        plan.append(up + [(0, row) for row in chunk if row >= edge])
    if rows_dev < WIN_R:
        return plan
    late = DEFER[layer]
    held = []
    for c, sends in enumerate(plan):
        ups = [send for send in sends if send[0] == 1]
        downs = held + [send for send in sends if send[0] == 0]
        held = downs[max(len(downs) - late[c], 0) :]
        plan[c] = ups + downs[: max(len(downs) - late[c], 0)]
    return plan


def row_groups(rows_dev, layer):
    every = list(range(rows_dev))
    below = HALO - 1 if rows_dev >= WIN_R else HALO
    edge, last = rows_dev - HALO, rows_dev - 1
    up = [(1, r) for r in range(below)]
    down = [(0, r) for r in range(edge, rows_dev)]
    if rows_dev < WIN_R:
        return [(up + down, every)]
    if layer == 0:
        return [
            ([(1, 0), (0, last)], every[3 : edge + 2]),
            ([(1, 1), (0, last - 1)], [2, last - 1]),
            ([(1, 2), (0, last - 2)], [1, last]),
            ([(0, edge)], [0]),
        ]
    return [(up, every[edge:]), (down, every[:edge])]


def kernel(
    n_sp,
    n_tp,
    x_ref,
    gain_a,
    gain_b,
    wq_a,
    wk_a,
    wv_a,
    wq_b,
    wk_b,
    wv_b,
    table_a,
    table_b,
    out_ref,
    xg_a,
    xg_b,
    w_a,
    w_b,
    kvp_a,
    kvp_b,
    q_buf,
    normed,
    gains_buf,
    tables_buf,
    rows_buf,
    tiles_a,
    tiles_b,
    load_sem,
    xs_sem,
    xr_sem,
    xp_sem,
    ws_sem,
    wr_sem,
    hs_sem,
    hr_sem,
):
    sp = lax.axis_index("sp")
    tp = lax.axis_index("tp")
    tokens, feat = x_ref.shape
    depth = wq_a.shape[0]
    rows_dev = tokens // GRID_W
    total_rows = rows_dev * n_sp
    half = n_tp // 2
    core = lax.rem(tp, 2)
    z = tp // 2
    partner = tp + 1 - 2 * core
    low = HALO * GRID_W
    below_rows = HALO - 1 if rows_dev >= WIN_R else HALO
    below = below_rows * GRID_W
    factor = feat ** (-0.5)
    orders = row_orders(rows_dev)
    chunks = len(orders[0])

    xg = (xg_a, xg_b)
    w = (w_a, w_b)
    kvp = (kvp_a, kvp_b)
    tiles = (tiles_a, tiles_b)

    square = n_sp == 4
    near_x = sp + 1 - 2 * lax.rem(sp, 2)
    near_y = lax.rem(sp + 2, n_sp)
    sp_peers = [lax.rem(sp + k, n_sp) for k in range(1, n_sp)]
    has_next = sp < n_sp - 1
    has_previous = sp > 0
    has_right = z < half - 1
    has_left = z > 0
    is_end = jnp.logical_not(has_left & has_right)
    crossed = (sp == 1) | (sp == 2)

    barrier = pltpu.get_barrier_semaphore()

    def greet(s, t):
        pl.semaphore_signal(barrier, inc=1, device_id=(s, t), device_id_type=MESH)

    pl.when(has_right)(lambda: greet(sp, tp + 2))
    pl.when(has_left)(lambda: greet(sp, tp - 2))
    for s in (near_x, near_y) if square else sp_peers:
        greet(s, tp)
    if square:
        pl.when(crossed)(lambda: greet(3 - sp, tp))
    greet(sp, partner)

    def slot_of(c, j):
        return c * half + j

    own = slot_of(core, z)

    def w_rows(device):
        return pl.ds(pl.multiple_of(device * depth, depth), depth)

    mine = w_rows(sp)

    flat = [[row for chunk in order for row in chunk] for order in orders]

    def place(layer, row):
        return flat[layer].index(row) * GRID_W + (GAIN_ROWS if layer == 0 else 0)

    def span(layer, c):
        at, size = place(layer, orders[layer][c][0]), len(orders[layer][c]) * GRID_W
        if layer == 0 and c == 0:
            return pl.ds(0, size + GAIN_ROWS)
        return pl.ds(at, size)

    runs = []
    for row in flat[0]:
        if runs and runs[-1][-1] == row - 1:
            runs[-1].append(row)
        else:
            runs.append([row])
    for run in runs:
        pltpu.make_async_copy(
            x_ref.at[pl.ds(run[0] * GRID_W, len(run) * GRID_W)],
            xg_a.at[own, pl.ds(place(0, run[0]), len(run) * GRID_W)],
            load_sem.at[0],
        ).start()
    loads = [
        (1, wk_a, w_a.at[mine, pl.ds(0, feat)]),
        (1, wv_a, w_a.at[mine, pl.ds(feat, feat)]),
        (1, wq_a, w_a.at[mine, pl.ds(2 * feat, feat)]),
        (3, gain_a, gains_buf.at[0]),
        (4, gain_b, gains_buf.at[1]),
        (5, table_a, tables_buf.at[0]),
        (6, table_b, tables_buf.at[1]),
        (2, wk_b, w_b.at[mine, pl.ds(0, feat)]),
        (2, wv_b, w_b.at[mine, pl.ds(feat, feat)]),
        (2, wq_b, w_b.at[mine, pl.ds(2 * feat, feat)]),
    ]
    for i, src, dst in loads:
        pltpu.make_async_copy(src, dst, load_sem.at[i]).start()

    def loaded(i, ref):
        pltpu.make_async_copy(ref, ref, load_sem.at[i]).wait()

    loaded(3, gains_buf.at[0])
    loaded(4, gains_buf.at[1])
    spare = jnp.zeros((GAIN_ROWS - 2, feat), jnp.float32)
    both = [gains_buf[0].astype(jnp.float32), gains_buf[1].astype(jnp.float32), spare]
    xg_a[own, 0:GAIN_ROWS, :] = jnp.concatenate(both, axis=0).astype(jnp.bfloat16)

    def remote(src, dst, send, recv, device):
        return pltpu.make_async_remote_copy(
            src_ref=src,
            dst_ref=dst,
            send_sem=send,
            recv_sem=recv,
            device_id=device,
            device_id_type=MESH,
        )

    def x_copy(layer, c, j, target):
        ref = xg[layer].at[slot_of(core, j), span(layer, c)]
        index = lax.rem(j - target + half, half) - 1
        device = (sp, 2 * target + core)
        return remote(ref, ref, xs_sem.at[layer], xr_sem.at[layer, c, index], device)

    def x_pass(layer, c, j):
        ref = xg[layer].at[slot_of(core, j), span(layer, c)]
        return remote(ref, ref, xs_sem.at[layer], xp_sem.at[layer, c], (sp, partner))

    def x_start(layer, c):
        for far in (2, 1)[c >= DIRECT[layer] :]:
            pl.when(z + far < half)(lambda far=far: x_copy(layer, c, z, z + far).start())
            pl.when(z - far >= 0)(lambda far=far: x_copy(layer, c, z, z - far).start())
        x_pass(layer, c, z).start()

    both_sides = jnp.minimum(z, half - 1 - z)
    far = jnp.where(2 * z < half, 1, -1)

    def source(k):
        paired = k <= 2 * both_sides
        away = jnp.where(paired, (k + 1) // 2, k - both_sides)
        side = jnp.where(paired, 1 if k % 2 else -1, far)
        return z + away * side, side, away

    sources = [source(k) for k in range(1, half)]

    def x_take(layer, c, k):
        j, side, away = sources[k - 1]
        index = lax.rem(j - z + half, half) - 1
        ref = xg[layer].at[slot_of(core, j), span(layer, c)]
        remote(ref, ref, xs_sem.at[layer], xr_sem.at[layer, c, index], (sp, partner)).wait_recv()
        onward = jnp.where(side > 0, has_left, has_right)
        if c < DIRECT[layer]:
            onward &= away >= 2
        pl.when(onward)(lambda: x_copy(layer, c, j, z - side).start())
        x_pass(layer, c, j).start()

    def x_finish(layer, c):
        ref = xg[layer].at[pl.ds((1 - core) * half, half), span(layer, c)]
        remote(ref, ref, xs_sem.at[layer], xp_sem.at[layer, c], (sp, partner)).wait_recv()

    def x_sent(layer, counts):
        for c, count in enumerate(counts):
            for part in [n_tp] * (count // n_tp) + [count % n_tp] * (count % n_tp > 0):
                ref = xg[layer].at[pl.ds(0, part), span(layer, c)]
                sems = xs_sem.at[layer], xp_sem.at[layer, 0]
                remote(ref, ref, *sems, (sp, partner)).wait_send()

    def x_drain(layer):
        for at in range(half):
            counts = []
            for c in range(chunks):
                reach = 2 if c < DIRECT[layer] else 1
                count = half
                for before, after in ((at, half - 1 - at), (half - 1 - at, at)):
                    count += min(reach, after) + (max(before - reach + 1, 0) if after else 0)
                counts.append(count)
            pl.when(z == at)(functools.partial(x_sent, layer, counts))

    def w_part(layer, device, which):
        size = depth // 2
        return w[layer].at[pl.ds(pl.multiple_of(device * depth + which * size, size), size)]

    def w_send(layer, ref, sem, target):
        remote(ref, ref, ws_sem.at[layer], wr_sem.at[layer, sem], (target, tp)).start()

    def w_start(layer, parts=(0, 1, 2, 3)):
        if not square:
            if 0 in parts:
                for target in sp_peers:
                    w_send(layer, w[layer].at[mine], 2, target)
            return
        plan = ((0, 0, near_x), (1, 1, near_y), (1, 2, near_x), (0, 2, near_y))
        for part in parts:
            which, sem, target = plan[part]
            w_send(layer, w_part(layer, sp, which), sem, target)

    def w_relay(layer, along=(0, 1)):
        if not square:
            return
        for which in along:
            source, target = ((near_x, near_y), (near_y, near_x))[which]
            ref = w_part(layer, source, which)
            sem = wr_sem.at[layer, which]
            remote(ref, ref, ws_sem.at[layer], sem, (source, tp)).wait_recv()
            w_send(layer, ref, 2, target)

    def w_all(layer, blocks):
        ref = w[layer].at[pl.ds(0, blocks * depth)]
        return remote(ref, ref, ws_sem.at[layer], wr_sem.at[layer, 2], (sp, partner))

    def halo(layer, way, row):
        buf = kvp[layer]
        target = lax.rem(sp + (1 if way == 0 else n_sp - 1), n_sp)
        at = low + row * GRID_W
        index = row - (rows_dev - HALO) if way == 0 else HALO + row
        return remote(
            buf.at[pl.ds(at, GRID_W)],
            buf.at[pl.ds(at + (tokens if way else -tokens), GRID_W)],
            hs_sem.at[layer, way],
            hr_sem.at[layer, index],
            (target, tp),
        )

    receives = (has_previous, has_next)

    def halo_start(layer, c):
        for way, row in halo_plan(rows_dev, layer)[c]:
            pl.when(receives[1 - way])(halo(layer, way, row).start)

    def halo_wait(layer, way, rows):
        pl.when(receives[way])(lambda: [halo(layer, way, row).wait_recv() for row in rows] and None)

    def halo_sent(layer, way):
        ref = kvp[layer].at[pl.ds(0, (low, below)[way])]
        copy = remote(ref, ref, hs_sem.at[layer, way], hr_sem.at[layer, 0], (sp, partner))
        pl.when(receives[1 - way])(copy.wait_send)

    def norm(layer, c):
        buf = xg[layer]
        for row in orders[layer][c]:
            at = pl.ds(place(layer, row), GRID_W)
            start = flat[layer].index(row) * GRID_W
            to = pl.ds(start, GRID_W)
            total = jnp.zeros((GRID_W, feat), jnp.float32)
            for s in range(n_tp):
                wide = buf[s, at, :].astype(jnp.float32)
                total = total + wide * wide
            mean = jnp.sum(total, axis=-1, keepdims=True) * (1.0 / (n_tp * feat))
            scale = lax.rsqrt(mean + epsilon)
            for s in range(n_tp):
                slot = slot_of(s % 2, s // 2)
                gain = xg_a[slot, 0:GAIN_ROWS, :][layer : layer + 1, :]
                wide = buf[slot, at, :].astype(jnp.float32)
                normed[to, s * feat : (s + 1) * feat] = (
                    wide * scale * gain.astype(jnp.float32)
                ).astype(jnp.bfloat16)

    def project(layer, c):
        chunk = orders[layer][c]
        at = flat[layer].index(chunk[0]) * GRID_W
        made = jnp.dot(
            normed[at : at + len(chunk) * GRID_W, :],
            w[layer][...],
            preferred_element_type=jnp.float32,
        ).astype(jnp.bfloat16)
        for i, row in enumerate(chunk):
            part = made[i * GRID_W : (i + 1) * GRID_W]
            to = row * GRID_W
            kvp[layer][low + to : low + to + GRID_W, :] = part[:, 0 : 2 * feat]
            q_buf[to : to + GRID_W, :] = part[:, 2 * feat : 3 * feat]
        halo_start(layer, c)

    def attend(layer, indices):
        places, scores = [], []
        for index in indices:
            row = sp * rows_dev + index
            first = jnp.minimum(jnp.maximum(row - HALO, 0), total_rows - WIN_R)
            local = first - sp * rows_dev + HALO
            base = first - row + WIN_R - 1
            at = pl.ds(pl.multiple_of(local * GRID_W, GRID_W), WIN_R * GRID_W)
            query = q_buf[index * GRID_W : (index + 1) * GRID_W, :]
            raw = lax.dot_general(
                query,
                kvp[layer][at, 0:feat],
                (((1,), (1,)), ((), ())),
                preferred_element_type=jnp.float32,
            )
            bias = jnp.concatenate([tiles[layer][base + 2 * j] for j in range(WIN_R // 2)], axis=1)
            places.append(at)
            scores.append(raw * factor + bias)
        tops = [jnp.max(score, axis=-1, keepdims=True) for score in scores]
        weights = [jnp.exp(score - top) for score, top in zip(scores, tops)]
        scales = [1.0 / jnp.sum(weight, axis=-1, keepdims=True) for weight in weights]
        outs = [
            jnp.dot(
                (weight * scale).astype(jnp.bfloat16),
                kvp[layer][at, feat : 2 * feat],
                preferred_element_type=jnp.float32,
            )
            for weight, scale, at in zip(weights, scales, places)
        ]
        made = []
        for index, out in zip(indices, outs):
            wide = xg[layer][own, pl.ds(place(layer, index), GRID_W), :].astype(jnp.float32)
            made.append((wide + out).astype(jnp.bfloat16))
        return made

    sync = 1 + has_right.astype(jnp.int32) + has_left.astype(jnp.int32)
    sync += 2 + crossed.astype(jnp.int32) if square else n_sp - 1
    pl.semaphore_wait(barrier, sync)
    loaded(0, xg_a.at[own, pl.ds(GAIN_ROWS, tokens)])
    for c in range(chunks):
        x_start(0, c)
    loaded(1, w_a.at[mine])
    w_start(0)
    loaded(5, tables_buf.at[0])
    loaded(6, tables_buf.at[1])
    build_bias(tables_buf.at[0], rows_buf, tiles_a)
    build_bias(tables_buf.at[1], rows_buf, tiles_b)
    loaded(2, w_b.at[mine])

    last = half - 1

    def lead_end(layer):
        if layer == 0:
            for c in range(chunks):
                x_take(layer, c, 1)
            w_relay(0)
            w_start(1, (0,))

    def end_take(layer, c):
        for k in range(2 - layer, last + 1):
            x_take(layer, c, k)

    def lead_middle(layer):
        for c in range(min(DIRECT[layer], chunks)):
            for k in range(1, last + 1):
                x_take(layer, c, k)
        for k in range(1, last + 1, 2):
            for c in range(DIRECT[layer], chunks):
                for one in range(k, min(k + 2, last + 1)):
                    x_take(layer, c, one)
            if k == 1 and layer == 0:
                w_relay(0)
        if layer == 0:
            w_start(1, (0,))

    for layer in range(2):
        pl.when(is_end)(functools.partial(lead_end, layer))
        if half > 2:
            pl.when(jnp.logical_not(is_end))(functools.partial(lead_middle, layer))
        lag = LAG[layer]
        for c in range(chunks + lag):
            if c < chunks:
                pl.when(is_end)(functools.partial(end_take, layer, c))
            if c < lag:
                continue
            x_finish(layer, c - lag)
            norm(layer, c - lag)
            if c == lag:
                if layer == 0 and square:
                    w_start(1, (1, 3))
                w_all(layer, 2 if square else n_sp - 1).wait_recv()
            project(layer, c - lag)

        finished, sent = set(), 0
        groups = row_groups(rows_dev, layer)
        for step, (waits, rows) in enumerate(groups):
            if layer == 0 and step == min(W_STEP, len(groups) - 1):
                if square:
                    w_start(1, (2,))
                w_relay(1)
            for way in range(2):
                asked = [row for each, row in waits if each == way]
                if asked:
                    halo_wait(layer, way, asked)
            for at in range(0, len(rows), BATCH):
                batch = rows[at : at + BATCH]
                for index, made in zip(batch, attend(layer, batch)):
                    if layer == 1:
                        out_ref[index * GRID_W : (index + 1) * GRID_W, :] = made
                    else:
                        xg_b[own, pl.ds(place(1, index), GRID_W), :] = made
                        finished.add(index)
                while layer == 0 and sent < chunks:
                    if not set(orders[1][sent]) <= finished:
                        break
                    x_start(1, sent)
                    sent += 1

    for layer in range(2):
        for way in range(2):
            halo_sent(layer, way)
        w_all(layer, n_sp - 1).wait_send()
        x_drain(layer)


def body(n_sp, n_tp, stream, gain_a, wq_a, wk_a, wv_a, table_a, gain_b, wq_b, wk_b, wv_b, table_b):
    tokens, feat = stream.shape
    depth = wq_a.shape[0] * n_sp
    rows_dev = tokens // GRID_W
    chunks = len(row_orders(rows_dev)[0])
    bf16 = jnp.bfloat16
    padded = tokens + 2 * HALO * GRID_W
    hbm = pl.BlockSpec(memory_space=pl.ANY)
    vmem = pl.BlockSpec(memory_space=pltpu.VMEM)
    dma = pltpu.SemaphoreType.DMA
    return pl.pallas_call(
        functools.partial(kernel, n_sp, n_tp),
        out_shape=pltpu.VMEM((tokens, feat), bf16),
        in_specs=[hbm] * 11,
        out_specs=vmem,
        scratch_shapes=[
            pltpu.VMEM((n_tp, tokens + GAIN_ROWS, feat), bf16),
            pltpu.VMEM((n_tp, tokens, feat), bf16),
            pltpu.VMEM((depth, 3 * feat), bf16),
            pltpu.VMEM((depth, 3 * feat), bf16),
            pltpu.VMEM((padded, 2 * feat), bf16),
            pltpu.VMEM((padded, 2 * feat), bf16),
            pltpu.VMEM((tokens, feat), bf16),
            pltpu.VMEM((tokens, n_tp * feat), bf16),
            pltpu.VMEM((2, 1, feat), bf16),
            pltpu.VMEM((2, 2 * WIN_R - 1, 1, 2 * WIN_C - 1), jnp.float32),
            pltpu.VMEM((2 * WIN_R, 2 * GRID_W), jnp.float32),
            pltpu.VMEM((2 * WIN_R - 2, GRID_W, 2 * GRID_W), jnp.float32),
            pltpu.VMEM((2 * WIN_R - 2, GRID_W, 2 * GRID_W), jnp.float32),
            dma((7,)),
            dma((2,)),
            dma((2, chunks, n_tp // 2 - 1)),
            dma((2, chunks)),
            dma((2,)),
            dma((2, 3)),
            dma((2, 2)),
            dma((2, 2 * HALO)),
        ],
        compiler_params=pltpu.CompilerParams(collective_id=0, has_side_effects=True),
    )(
        stream,
        gain_a.reshape(1, feat),
        gain_b.reshape(1, feat),
        wq_a,
        wk_a,
        wv_a,
        wq_b,
        wk_b,
        wv_b,
        jnp.transpose(table_a, (1, 0, 2)),
        jnp.transpose(table_b, (1, 0, 2)),
    )


def solution(mesh):
    placed = (
        P("sp", "tp"),
        P("tp"),
        P("sp", "tp"),
        P("sp", "tp"),
        P("sp", "tp"),
        P("tp", None, None),
        P("tp"),
        P("sp", "tp"),
        P("sp", "tp"),
        P("sp", "tp"),
        P("tp", None, None),
    )
    return jax.shard_map(
        functools.partial(body, mesh.shape["sp"], mesh.shape["tp"]),
        mesh=mesh,
        in_specs=placed,
        out_specs=P("sp", "tp"),
        check_vma=False,
    )
```

time: 43.3 us -> 37.2 us (0.86)
  the two profiles are of different devices: /device:TPU:0 before, /device:TPU:5 now
where the time goes in v2:
time: 37.2 us; the launch traced here: 37.1 us
  Pallas kernels  36.4 us (98%)
  local copies, waits for them, and re-layouts  0.66 us (2%)
    pallas_call x1, Pallas kernels, body(): pl.pallas_call(functools.partial(kernel, n_sp, n_tp), out_shape=pltpu.VME...  36.4 us

profile of v2, /device:TPU:5, one launch (start us, length us, event | category | flops | bytes accessed | tf_op | source)
XLA Modules:
  0.0 37.1 jit_solution(6609423446686327523)
XLA Ops:
  0.0 36.4 %shard_map.109 = bf16[512,128]{1,0:T(8,128)(2,1)S(1)} custom-call(bf16[512,128]{1,0:T(8,128)(2,1)} %x_ref.1, bf16[1,128]{1,0:T(2,128)(2,1)} %bitcast.6, bf16[1,128]{1,0:T(2,128)(2,1)} %bitcast.7, bf16[256,128]{1,0:T(8,128)(2,1)} %wq_a.1, bf16[256,128]{1,0:T(8,128)(2,1)} %wk_a.1, bf16[256,128]{1,0:T(8,128)(2,1)} %wv_a.1, bf16[256,128]{1,0:T(8,128)(2,1)} %wq_b.1, ...), custom_call_target="tpu_custom_call" | custom-call | tf_op jit(solution)/shard_map/pallas_call | solution.py:527
  36.4 0.7 %copy.13 = bf16[512,128]{1,0:T(8,128)(2,1)} copy(bf16[512,128]{1,0:T(8,128)(2,1)S(1)} %shard_map.109) | data formatting | bytes 262144

commit v3 on v2

--- a/solution.py
+++ b/solution.py
@@ -12,11 +12,16 @@
 WIN_C = 16
 HALO = 4
 GAIN_ROWS = 16
-LAG = (1, 1)
-DIRECT = (0, 4)
+LAG = (2, 1)
+EAGER = (1, 0)
+DIRECT = (1, 4)
+ENDS = (1, 1)
 DEFER = ((0, 0, 0, 0), (1, 2, 3, 0))
-BATCH = 4
+BATCH = 5
 W_STEP = 2
+W_EARLY = 0
+SWAP = (False, True)
+PACE = (1, 2, 3)
 epsilon = 1e-06
 MESH = pl.DeviceIdType.MESH
 
@@ -82,7 +87,7 @@
             ([(1, 2), (0, last - 2)], [1, last]),
             ([(0, edge)], [0]),
         ]
-    return [(up, every[edge:]), (down, every[:edge])]
+    return [([], [edge]), (up, every[edge + 1 :]), (down, every[:edge])]
 
 
 def kernel(
@@ -114,12 +119,10 @@
     tiles_a,
     tiles_b,
     load_sem,
-    xs_sem,
+    send_sem,
     xr_sem,
     xp_sem,
-    ws_sem,
     wr_sem,
-    hs_sem,
     hr_sem,
 ):
     sp = lax.axis_index("sp")
@@ -137,7 +140,7 @@
     below = below_rows * GRID_W
     factor = feat ** (-0.5)
     orders = row_orders(rows_dev)
-    chunks = len(orders[0])
+    counts = [len(order) for order in orders]
 
     xg = (xg_a, xg_b)
     w = (w_a, w_b)
@@ -162,6 +165,10 @@
 
     pl.when(has_right)(lambda: greet(sp, tp + 2))
     pl.when(has_left)(lambda: greet(sp, tp - 2))
+    if DIRECT[0] and half > 2:
+        pl.when(z == half - 3)(lambda: greet(sp, tp + 4))
+        if ENDS[0] == 1:
+            pl.when(z == 2)(lambda: greet(sp, tp - 4))
     for s in (near_x, near_y) if square else sp_peers:
         greet(s, tp)
     if square:
@@ -206,9 +213,9 @@
         (1, wv_a, w_a.at[mine, pl.ds(feat, feat)]),
         (1, wq_a, w_a.at[mine, pl.ds(2 * feat, feat)]),
         (3, gain_a, gains_buf.at[0]),
-        (4, gain_b, gains_buf.at[1]),
-        (5, table_a, tables_buf.at[0]),
-        (6, table_b, tables_buf.at[1]),
+        (3, gain_b, gains_buf.at[1]),
+        (4, table_a, tables_buf.at[0]),
+        (4, table_b, tables_buf.at[1]),
         (2, wk_b, w_b.at[mine, pl.ds(0, feat)]),
         (2, wv_b, w_b.at[mine, pl.ds(feat, feat)]),
         (2, wq_b, w_b.at[mine, pl.ds(2 * feat, feat)]),
@@ -219,8 +226,7 @@
     def loaded(i, ref):
         pltpu.make_async_copy(ref, ref, load_sem.at[i]).wait()
 
-    loaded(3, gains_buf.at[0])
-    loaded(4, gains_buf.at[1])
+    loaded(3, gains_buf)
     spare = jnp.zeros((GAIN_ROWS - 2, feat), jnp.float32)
     both = [gains_buf[0].astype(jnp.float32), gains_buf[1].astype(jnp.float32), spare]
     xg_a[own, 0:GAIN_ROWS, :] = jnp.concatenate(both, axis=0).astype(jnp.bfloat16)
@@ -239,16 +245,25 @@
         ref = xg[layer].at[slot_of(core, j), span(layer, c)]
         index = lax.rem(j - target + half, half) - 1
         device = (sp, 2 * target + core)
-        return remote(ref, ref, xs_sem.at[layer], xr_sem.at[layer, c, index], device)
+        return remote(ref, ref, send_sem, xr_sem.at[layer, c, index], device)
 
     def x_pass(layer, c, j):
         ref = xg[layer].at[slot_of(core, j), span(layer, c)]
-        return remote(ref, ref, xs_sem.at[layer], xp_sem.at[layer, c], (sp, partner))
+        return remote(ref, ref, send_sem, xp_sem.at[layer, c], (sp, partner))
+
+    def reaches(layer, c, j):
+        senders = (True, (j == 0) | (j == half - 1), j == half - 1)[ENDS[layer]]
+        return (c < DIRECT[layer]) & senders
 
     def x_start(layer, c):
         for far in (2, 1)[c >= DIRECT[layer] :]:
-            pl.when(z + far < half)(lambda far=far: x_copy(layer, c, z, z + far).start())
-            pl.when(z - far >= 0)(lambda far=far: x_copy(layer, c, z, z - far).start())
+            allowed = reaches(layer, c, z) if far == 2 else True
+            pl.when((z + far < half) & allowed)(
+                lambda far=far: x_copy(layer, c, z, z + far).start()
+            )
+            pl.when((z - far >= 0) & allowed)(
+                lambda far=far: x_copy(layer, c, z, z - far).start()
+            )
         x_pass(layer, c, z).start()
 
     both_sides = jnp.minimum(z, half - 1 - z)
@@ -257,7 +272,7 @@
     def source(k):
         paired = k <= 2 * both_sides
         away = jnp.where(paired, (k + 1) // 2, k - both_sides)
-        side = jnp.where(paired, 1 if k % 2 else -1, far)
+        side = far if k % 2 else jnp.where(paired, -far, far)
         return z + away * side, side, away
 
     sources = [source(k) for k in range(1, half)]
@@ -266,41 +281,45 @@
         j, side, away = sources[k - 1]
         index = lax.rem(j - z + half, half) - 1
         ref = xg[layer].at[slot_of(core, j), span(layer, c)]
-        remote(ref, ref, xs_sem.at[layer], xr_sem.at[layer, c, index], (sp, partner)).wait_recv()
+        remote(ref, ref, send_sem, xr_sem.at[layer, c, index], (sp, partner)).wait_recv()
         onward = jnp.where(side > 0, has_left, has_right)
         if c < DIRECT[layer]:
-            onward &= away >= 2
+            onward &= (away >= 2) | jnp.logical_not(reaches(layer, c, j))
         pl.when(onward)(lambda: x_copy(layer, c, j, z - side).start())
         x_pass(layer, c, j).start()
 
     def x_finish(layer, c):
         ref = xg[layer].at[pl.ds((1 - core) * half, half), span(layer, c)]
-        remote(ref, ref, xs_sem.at[layer], xp_sem.at[layer, c], (sp, partner)).wait_recv()
-
-    def x_sent(layer, counts):
-        for c, count in enumerate(counts):
+        remote(ref, ref, send_sem, xp_sem.at[layer, c], (sp, partner)).wait_recv()
+
+    def x_sent(layer, totals):
+        for c, count in enumerate(totals):
             for part in [n_tp] * (count // n_tp) + [count % n_tp] * (count % n_tp > 0):
                 ref = xg[layer].at[pl.ds(0, part), span(layer, c)]
-                sems = xs_sem.at[layer], xp_sem.at[layer, 0]
+                sems = send_sem, xp_sem.at[layer, 0]
                 remote(ref, ref, *sems, (sp, partner)).wait_send()
 
     def x_drain(layer):
         for at in range(half):
-            counts = []
-            for c in range(chunks):
-                reach = 2 if c < DIRECT[layer] else 1
+            totals = []
+            for c in range(counts[layer]):
                 count = half
-                for before, after in ((at, half - 1 - at), (half - 1 - at, at)):
-                    count += min(reach, after) + (max(before - reach + 1, 0) if after else 0)
-                counts.append(count)
-            pl.when(z == at)(functools.partial(x_sent, layer, counts))
+                for j in range(half):
+                    direct = bool(reaches(layer, c, j))
+                    for way in (-1, 1):
+                        if not 0 <= at + way < half or (at - j) * way < 0:
+                            continue
+                        count += not (direct and abs(at - j) == 1)
+                        count += direct and j == at and 0 <= at + 2 * way < half
+                totals.append(count)
+            pl.when(z == at)(functools.partial(x_sent, layer, totals))
 
     def w_part(layer, device, which):
         size = depth // 2
         return w[layer].at[pl.ds(pl.multiple_of(device * depth + which * size, size), size)]
 
     def w_send(layer, ref, sem, target):
-        remote(ref, ref, ws_sem.at[layer], wr_sem.at[layer, sem], (target, tp)).start()
+        remote(ref, ref, send_sem, wr_sem.at[layer, sem], (target, tp)).start()
 
     def w_start(layer, parts=(0, 1, 2, 3)):
         if not square:
@@ -320,23 +339,25 @@
             source, target = ((near_x, near_y), (near_y, near_x))[which]
             ref = w_part(layer, source, which)
             sem = wr_sem.at[layer, which]
-            remote(ref, ref, ws_sem.at[layer], sem, (source, tp)).wait_recv()
+            remote(ref, ref, send_sem, sem, (source, tp)).wait_recv()
             w_send(layer, ref, 2, target)
 
     def w_all(layer, blocks):
         ref = w[layer].at[pl.ds(0, blocks * depth)]
-        return remote(ref, ref, ws_sem.at[layer], wr_sem.at[layer, 2], (sp, partner))
+        return remote(ref, ref, send_sem, wr_sem.at[layer, 2], (sp, partner))
 
     def halo(layer, way, row):
         buf = kvp[layer]
         target = lax.rem(sp + (1 if way == 0 else n_sp - 1), n_sp)
         at = low + row * GRID_W
         index = row - (rows_dev - HALO) if way == 0 else HALO + row
+        if layer == 1:
+            index = 2 * HALO + way
         return remote(
             buf.at[pl.ds(at, GRID_W)],
             buf.at[pl.ds(at + (tokens if way else -tokens), GRID_W)],
-            hs_sem.at[layer, way],
-            hr_sem.at[layer, index],
+            send_sem,
+            hr_sem.at[index],
             (target, tp),
         )
 
@@ -347,11 +368,22 @@
             pl.when(receives[1 - way])(halo(layer, way, row).start)
 
     def halo_wait(layer, way, rows):
-        pl.when(receives[way])(lambda: [halo(layer, way, row).wait_recv() for row in rows] and None)
+        if layer == 0:
+            copies = [halo(layer, way, row) for row in rows]
+        else:
+            at, size = ((0, low), (low + tokens, below))[way]
+            ref = kvp[layer].at[pl.ds(at, size)]
+            copies = [remote(ref, ref, send_sem, hr_sem.at[2 * HALO + way], (sp, partner))]
+
+        def wait():
+            for copy in copies:
+                copy.wait_recv()
+
+        pl.when(receives[way])(wait)
 
     def halo_sent(layer, way):
         ref = kvp[layer].at[pl.ds(0, (low, below)[way])]
-        copy = remote(ref, ref, hs_sem.at[layer, way], hr_sem.at[layer, 0], (sp, partner))
+        copy = remote(ref, ref, send_sem, hr_sem.at[0], (sp, partner))
         pl.when(receives[1 - way])(copy.wait_send)
 
     def norm(layer, c):
@@ -426,23 +458,32 @@
 
     sync = 1 + has_right.astype(jnp.int32) + has_left.astype(jnp.int32)
     sync += 2 + crossed.astype(jnp.int32) if square else n_sp - 1
+    if DIRECT[0] and half > 2:
+        sync += (z == half - 1).astype(jnp.int32)
+        if ENDS[0] == 1:
+            sync += (z == 0).astype(jnp.int32)
     pl.semaphore_wait(barrier, sync)
     loaded(0, xg_a.at[own, pl.ds(GAIN_ROWS, tokens)])
-    for c in range(chunks):
+    x_start(0, 0)
+    spread = [min(at, counts[0]) for at in PACE]
+    for c in range(spread[0], spread[1]):
         x_start(0, c)
     loaded(1, w_a.at[mine])
     w_start(0)
-    loaded(5, tables_buf.at[0])
-    loaded(6, tables_buf.at[1])
+    loaded(4, tables_buf)
     build_bias(tables_buf.at[0], rows_buf, tiles_a)
+    for c in range(spread[1], spread[2]):
+        x_start(0, c)
     build_bias(tables_buf.at[1], rows_buf, tiles_b)
+    for c in range(spread[2], counts[0]):
+        x_start(0, c)
     loaded(2, w_b.at[mine])
 
     last = half - 1
 
     def lead_end(layer):
         if layer == 0:
-            for c in range(chunks):
+            for c in range(counts[0]):
                 x_take(layer, c, 1)
             w_relay(0)
             w_start(1, (0,))
@@ -452,39 +493,62 @@
             x_take(layer, c, k)
 
     def lead_middle(layer):
-        for c in range(min(DIRECT[layer], chunks)):
+        straight = min(DIRECT[layer], counts[layer])
+        late = [2] if SWAP[layer] and last == 3 else []
+        for c in range(straight):
             for k in range(1, last + 1):
-                x_take(layer, c, k)
+                if k not in late:
+                    x_take(layer, c, k)
         for k in range(1, last + 1, 2):
-            for c in range(DIRECT[layer], chunks):
+            for c in range(straight, counts[layer]):
                 for one in range(k, min(k + 2, last + 1)):
                     x_take(layer, c, one)
             if k == 1 and layer == 0:
                 w_relay(0)
-        if layer == 0:
+        for c in range(straight):
+            for k in late:
+                x_take(layer, c, k)
+        if layer == 0 and W_EARLY == 0:
             w_start(1, (0,))
+
+    def handle(layer, rows):
+        for at in range(0, len(rows), BATCH):
+            batch = rows[at : at + BATCH]
+            for index, made in zip(batch, attend(layer, batch)):
+                if layer == 1:
+                    out_ref[index * GRID_W : (index + 1) * GRID_W, :] = made
+                else:
+                    xg_b[own, pl.ds(place(1, index), GRID_W), :] = made
 
     for layer in range(2):
         pl.when(is_end)(functools.partial(lead_end, layer))
         if half > 2:
             pl.when(jnp.logical_not(is_end))(functools.partial(lead_middle, layer))
-        lag = LAG[layer]
-        for c in range(chunks + lag):
-            if c < chunks:
+        lag, chunks = LAG[layer], counts[layer]
+        steps, made = [], 0
+        for c in range(chunks):
+            steps.append((True, c))
+            while made <= (c if made < EAGER[layer] else c - lag):
+                steps.append((False, made))
+                made += 1
+        steps += [(False, c) for c in range(made, chunks)]
+        for taking, c in steps:
+            if taking:
                 pl.when(is_end)(functools.partial(end_take, layer, c))
-            if c < lag:
                 continue
-            x_finish(layer, c - lag)
-            norm(layer, c - lag)
-            if c == lag:
+            x_finish(layer, c)
+            norm(layer, c)
+            if c == 0:
                 if layer == 0 and square:
                     w_start(1, (1, 3))
                 w_all(layer, 2 if square else n_sp - 1).wait_recv()
-            project(layer, c - lag)
+            project(layer, c)
 
         finished, sent = set(), 0
         groups = row_groups(rows_dev, layer)
         for step, (waits, rows) in enumerate(groups):
+            if layer == 0 and step == W_EARLY - 1 and half > 2:
+                pl.when(jnp.logical_not(is_end))(functools.partial(w_start, 1, (0,)))
             if layer == 0 and step == min(W_STEP, len(groups) - 1):
                 if square:
                     w_start(1, (2,))
@@ -493,19 +557,22 @@
                 asked = [row for each, row in waits if each == way]
                 if asked:
                     halo_wait(layer, way, asked)
-            for at in range(0, len(rows), BATCH):
-                batch = rows[at : at + BATCH]
-                for index, made in zip(batch, attend(layer, batch)):
-                    if layer == 1:
-                        out_ref[index * GRID_W : (index + 1) * GRID_W, :] = made
-                    else:
-                        xg_b[own, pl.ds(place(1, index), GRID_W), :] = made
-                        finished.add(index)
-                while layer == 0 and sent < chunks:
-                    if not set(orders[1][sent]) <= finished:
-                        break
-                    x_start(1, sent)
-                    sent += 1
+            if layer == 0 or rows_dev < WIN_R:
+                handle(layer, rows)
+            elif step == 0:
+                pl.when(has_previous)(functools.partial(handle, layer, rows))
+                ahead = groups[2][1] + rows
+                pl.when(jnp.logical_not(has_previous))(functools.partial(handle, layer, ahead))
+            elif step == 1:
+                handle(layer, rows)
+            else:
+                pl.when(has_previous)(functools.partial(handle, layer, rows))
+            finished |= set(rows)
+            while layer == 0 and sent < counts[1]:
+                if not set(orders[1][sent]) <= finished:
+                    break
+                x_start(1, sent)
+                sent += 1
 
     for layer in range(2):
         for way in range(2):
@@ -518,7 +585,7 @@
     tokens, feat = stream.shape
     depth = wq_a.shape[0] * n_sp
     rows_dev = tokens // GRID_W
-    chunks = len(row_orders(rows_dev)[0])
+    chunks = max(len(order) for order in row_orders(rows_dev))
     bf16 = jnp.bfloat16
     padded = tokens + 2 * HALO * GRID_W
     hbm = pl.BlockSpec(memory_space=pl.ANY)
@@ -543,14 +610,12 @@
             pltpu.VMEM((2 * WIN_R, 2 * GRID_W), jnp.float32),
             pltpu.VMEM((2 * WIN_R - 2, GRID_W, 2 * GRID_W), jnp.float32),
             pltpu.VMEM((2 * WIN_R - 2, GRID_W, 2 * GRID_W), jnp.float32),
-            dma((7,)),
-            dma((2,)),
+            dma((5,)),
+            dma,
             dma((2, chunks, n_tp // 2 - 1)),
             dma((2, chunks)),
-            dma((2,)),
             dma((2, 3)),
-            dma((2, 2)),
-            dma((2, 2 * HALO)),
+            dma((2 * HALO + 2,)),
         ],
         compiler_params=pltpu.CompilerParams(collective_id=0, has_side_effects=True),
     )(

time: 37.2 us -> 36.1 us (0.970)
  Pallas kernels: 36.4 us -> 35 us
    pallas_call x1, Pallas kernels: 36.4 us -> 35 us  [body(): pl.pallas_call(functools.partial(kernel, n_sp, n_tp), out_shape=pltpu.VME...]
where the time goes in v3:
time: 36.1 us; the launch traced here: 35.7 us
  Pallas kernels  35 us (97%)
  local copies, waits for them, and re-layouts  0.66 us (2%)
    pallas_call x1, Pallas kernels, body(): pl.pallas_call(functools.partial(kernel, n_sp, n_tp), out_shape=pltpu.VME...  35 us

profile of v3, /device:TPU:5, one launch (start us, length us, event | category | flops | bytes accessed | tf_op | source)
XLA Modules:
  0.0 35.7 jit_solution(14229103972160732278)
XLA Ops:
  0.0 35.0 %shard_map.109 = bf16[512,128]{1,0:T(8,128)(2,1)S(1)} custom-call(bf16[512,128]{1,0:T(8,128)(2,1)} %x_ref.1, bf16[1,128]{1,0:T(2,128)(2,1)} %bitcast.6, bf16[1,128]{1,0:T(2,128)(2,1)} %bitcast.7, bf16[256,128]{1,0:T(8,128)(2,1)} %wq_a.1, bf16[256,128]{1,0:T(8,128)(2,1)} %wk_a.1, bf16[256,128]{1,0:T(8,128)(2,1)} %wv_a.1, bf16[256,128]{1,0:T(8,128)(2,1)} %wq_b.1, ...), custom_call_target="tpu_custom_call" | custom-call | tf_op jit(solution)/shard_map/pallas_call | solution.py:594
  35.1 0.7 %copy.13 = bf16[512,128]{1,0:T(8,128)(2,1)} copy(bf16[512,128]{1,0:T(8,128)(2,1)S(1)} %shard_map.109) | data formatting | bytes 262144

commit v4 on v3

--- a/solution.py
+++ b/solution.py
@@ -12,8 +12,7 @@
 WIN_C = 16
 HALO = 4
 GAIN_ROWS = 16
-LAG = (2, 1)
-EAGER = (1, 0)
+AHEAD = (((1, 4, 4, 4), (1, 4, 4, 4)), ((1, 2, 3, 4), (3, 4, 4, 4)))
 DIRECT = (1, 4)
 ENDS = (1, 1)
 DEFER = ((0, 0, 0, 0), (1, 2, 3, 0))
@@ -23,6 +22,7 @@
 SWAP = (False, True)
 PACE = (1, 2, 3)
 epsilon = 1e-06
+LOG2E = 1.4426950408889634
 MESH = pl.DeviceIdType.MESH
 
 
@@ -40,7 +40,7 @@
         tile = pltpu.roll(
             jnp.broadcast_to(pair, shape), 2 * GRID_W - (WIN_C - 1), 1, stride=1, stride_axis=0
         )
-        tiles_ref[o] = jnp.where(inside, tile, -1e30)
+        tiles_ref[o] = jnp.where(inside, tile * LOG2E, -1e30)
 
 
 def row_orders(rows_dev):
@@ -138,7 +138,7 @@
     low = HALO * GRID_W
     below_rows = HALO - 1 if rows_dev >= WIN_R else HALO
     below = below_rows * GRID_W
-    factor = feat ** (-0.5)
+    factor = feat ** (-0.5) * LOG2E
     orders = row_orders(rows_dev)
     counts = [len(order) for order in orders]
 
@@ -440,20 +440,20 @@
             places.append(at)
             scores.append(raw * factor + bias)
         tops = [jnp.max(score, axis=-1, keepdims=True) for score in scores]
-        weights = [jnp.exp(score - top) for score, top in zip(scores, tops)]
-        scales = [1.0 / jnp.sum(weight, axis=-1, keepdims=True) for weight in weights]
+        weights = [jnp.exp2(score - top) for score, top in zip(scores, tops)]
         outs = [
             jnp.dot(
-                (weight * scale).astype(jnp.bfloat16),
+                weight.astype(jnp.bfloat16),
                 kvp[layer][at, feat : 2 * feat],
                 preferred_element_type=jnp.float32,
             )
-            for weight, scale, at in zip(weights, scales, places)
+            for weight, at in zip(weights, places)
         ]
+        scales = [1.0 / jnp.sum(weight, axis=-1, keepdims=True) for weight in weights]
         made = []
-        for index, out in zip(indices, outs):
+        for index, out, scale in zip(indices, outs, scales):
             wide = xg[layer][own, pl.ds(place(layer, index), GRID_W), :].astype(jnp.float32)
-            made.append((wide + out).astype(jnp.bfloat16))
+            made.append((wide + out * scale).astype(jnp.bfloat16))
         return made
 
     sync = 1 + has_right.astype(jnp.int32) + has_left.astype(jnp.int32)
@@ -524,18 +524,15 @@
         pl.when(is_end)(functools.partial(lead_end, layer))
         if half > 2:
             pl.when(jnp.logical_not(is_end))(functools.partial(lead_middle, layer))
-        lag, chunks = LAG[layer], counts[layer]
-        steps, made = [], 0
+        chunks = counts[layer]
+        taken = [0, 0]
         for c in range(chunks):
-            steps.append((True, c))
-            while made <= (c if made < EAGER[layer] else c - lag):
-                steps.append((False, made))
-                made += 1
-        steps += [(False, c) for c in range(made, chunks)]
-        for taking, c in steps:
-            if taking:
-                pl.when(is_end)(functools.partial(end_take, layer, c))
-                continue
+            for side in range(2):
+                stop = min(AHEAD[layer][side][min(c, 3)], chunks) if chunks == 4 else c + 1
+                for ask in range(taken[side], stop):
+                    mine_now = is_end & (core == side)
+                    pl.when(mine_now)(functools.partial(end_take, layer, ask))
+                taken[side] = max(taken[side], stop)
             x_finish(layer, c)
             norm(layer, c)
             if c == 0:
@@ -543,6 +540,33 @@
                     w_start(1, (1, 3))
                 w_all(layer, 2 if square else n_sp - 1).wait_recv()
             project(layer, c)
+
+        if layer == 1 and rows_dev >= WIN_R:
+            (_, middle), (up, above), (down, under) = row_groups(rows_dev, layer)
+            low_first = sp <= n_sp // 4
+
+            def finish_low():
+                handle(layer, under + middle)
+
+            def finish_high():
+                handle(layer, middle)
+
+            ask_down = functools.partial(halo_wait, layer, 0, [row for _, row in down])
+
+            def low_side():
+                ask_down()
+                finish_low()
+
+            def high_side():
+                ask_down()
+                handle(layer, under)
+
+            pl.when(low_first)(low_side)
+            pl.when(jnp.logical_not(low_first))(finish_high)
+            halo_wait(layer, 1, [row for _, row in up])
+            handle(layer, above)
+            pl.when(jnp.logical_not(low_first))(high_side)
+            continue
 
         finished, sent = set(), 0
         groups = row_groups(rows_dev, layer)
@@ -557,16 +581,7 @@
                 asked = [row for each, row in waits if each == way]
                 if asked:
                     halo_wait(layer, way, asked)
-            if layer == 0 or rows_dev < WIN_R:
-                handle(layer, rows)
-            elif step == 0:
-                pl.when(has_previous)(functools.partial(handle, layer, rows))
-                ahead = groups[2][1] + rows
-                pl.when(jnp.logical_not(has_previous))(functools.partial(handle, layer, ahead))
-            elif step == 1:
-                handle(layer, rows)
-            else:
-                pl.when(has_previous)(functools.partial(handle, layer, rows))
+            handle(layer, rows)
             finished |= set(rows)
             while layer == 0 and sent < counts[1]:
                 if not set(orders[1][sent]) <= finished:

time: 36.1 us -> 35.9 us (level)
  no operation moved by 1% of the time
where the time goes in v4:
time: 35.9 us; the launch traced here: 35.7 us
  Pallas kernels  35 us (97%)
  local copies, waits for them, and re-layouts  0.66 us (2%)
    pallas_call x1, Pallas kernels, body(): pl.pallas_call(functools.partial(kernel, n_sp, n_tp), out_shape=pltpu.VME...  35 us

profile of v4, /device:TPU:5, one launch (start us, length us, event | category | flops | bytes accessed | tf_op | source)
XLA Modules:
  0.0 35.7 jit_solution(1334598647806771743)
XLA Ops:
  0.0 35.0 %shard_map.109 = bf16[512,128]{1,0:T(8,128)(2,1)S(1)} custom-call(bf16[512,128]{1,0:T(8,128)(2,1)} %x_ref.1, bf16[1,128]{1,0:T(2,128)(2,1)} %bitcast.6, bf16[1,128]{1,0:T(2,128)(2,1)} %bitcast.7, bf16[256,128]{1,0:T(8,128)(2,1)} %wq_a.1, bf16[256,128]{1,0:T(8,128)(2,1)} %wk_a.1, bf16[256,128]{1,0:T(8,128)(2,1)} %wv_a.1, bf16[256,128]{1,0:T(8,128)(2,1)} %wq_b.1, ...), custom_call_target="tpu_custom_call" | custom-call | tf_op jit(solution)/shard_map/pallas_call | solution.py:609
  35.0 0.7 %copy.13 = bf16[512,128]{1,0:T(8,128)(2,1)} copy(bf16[512,128]{1,0:T(8,128)(2,1)S(1)} %shard_map.109) | data formatting | bytes 262144

commit v5 on v4

--- a/solution.py
+++ b/solution.py
@@ -536,9 +536,9 @@
             x_finish(layer, c)
             norm(layer, c)
             if c == 0:
+                w_all(layer, 2 if square else n_sp - 1).wait_recv()
                 if layer == 0 and square:
                     w_start(1, (1, 3))
-                w_all(layer, 2 if square else n_sp - 1).wait_recv()
             project(layer, c)
 
         if layer == 1 and rows_dev >= WIN_R:

time: 35.9 us -> 35.9 us (level)
  no operation moved by 1% of the time
where the time goes in v5:
time: 35.9 us; the launch traced here: 35.7 us
  Pallas kernels  35 us (97%)
  local copies, waits for them, and re-layouts  0.66 us (2%)
    pallas_call x1, Pallas kernels, body(): pl.pallas_call(functools.partial(kernel, n_sp, n_tp), out_shape=pltpu.VME...  35 us

profile of v5, /device:TPU:5, one launch (start us, length us, event | category | flops | bytes accessed | tf_op | source)
XLA Modules:
  0.0 35.7 jit_solution(6766600028019431654)
XLA Ops:
  0.0 35.0 %shard_map.109 = bf16[512,128]{1,0:T(8,128)(2,1)S(1)} custom-call(bf16[512,128]{1,0:T(8,128)(2,1)} %x_ref.1, bf16[1,128]{1,0:T(2,128)(2,1)} %bitcast.6, bf16[1,128]{1,0:T(2,128)(2,1)} %bitcast.7, bf16[256,128]{1,0:T(8,128)(2,1)} %wq_a.1, bf16[256,128]{1,0:T(8,128)(2,1)} %wk_a.1, bf16[256,128]{1,0:T(8,128)(2,1)} %wv_a.1, bf16[256,128]{1,0:T(8,128)(2,1)} %wq_b.1, ...), custom_call_target="tpu_custom_call" | custom-call | tf_op jit(solution)/shard_map/pallas_call | solution.py:609
  35.0 0.7 %copy.13 = bf16[512,128]{1,0:T(8,128)(2,1)} copy(bf16[512,128]{1,0:T(8,128)(2,1)S(1)} %shard_map.109) | data formatting | bytes 262144
